TPU v7x, 32 devices: a whole 2x2x4 slice. The times are simulated.
32 devices in a mesh: dp: 4 (over y, x), kv: 4 (over z), tp: 2 (over core).
Axes of the slice: x: 2, y: 2, z: 4, core: 2. Of those that a mesh axis runs over, the one named last changes fastest.
Arguments:
- token_state: bfloat16 [64, 4096], P('dp', 'kv'), may hold values from -150 to 150
- norm_gain: float32 [4096], P('kv'), may hold values from 0.1 to 1.9
- wq_nope: bfloat16 [4096, 1024], P('kv', 'tp'), may hold values from -0.09375 to 0.09375
- wq_rope: bfloat16 [4096, 512], P('kv', 'tp'), may hold values from -0.09375 to 0.09375
- w_latent: bfloat16 [4096, 512], P('kv'), may hold values from -0.09375 to 0.09375
- w_rope_key: bfloat16 [4096, 32], P('kv'), may hold values from -0.09375 to 0.09375
- kv_gain: float32 [512], replicated, may hold values from 0.1 to 1.9
- w_uk: bfloat16 [512, 1024], P('kv', 'tp'), may hold values from -0.25 to 0.25
- w_uv: bfloat16 [512, 1024], P('kv', 'tp'), may hold values from -6 to 6
- w_out: bfloat16 [1024, 4096], P('tp', 'kv'), may hold values from -0.1875 to 0.1875
- latent_cache: bfloat16 [64, 768, 512], P('dp', 'kv'), may hold values from -500 to 500
- rope_cache: bfloat16 [64, 32, 768], P('dp', None, 'kv'), may hold values from -6 to 6
- lengths: int32 [64], P('dp'), may hold values from 192 to 767, as said below
Outputs:
- mixed: bfloat16 [64, 4096], P('dp', ('kv', 'tp'))
- latent_new: bfloat16 [64, 512], P('dp')
- rope_new: bfloat16 [64, 32], P('dp')
Inputs may be any that keep to these rules, and one draw needn't show every extreme that they name: Sequence b has cached positions 0 to lengths[b] - 1 and its new token takes position lengths[b]; in each aligned block of 16 sequences one has length 767.
All inputs are finite; a program needn't handle non-finite values.
Results may differ from a plain program's by a relative error of at most 0.02.
Values may be sent and summed in bfloat16 or wider, within the bound.
A program may use at most 64 MiB of HBM per device.

v0:
```python
import jax
import jax.numpy as jnp
from jax import lax
from jax.sharding import PartitionSpec as P

D = 4096
NOPE = 64
ROPE = 32
V_DIM = 64


EPS = 1e-06
THETA = 10000.0
NEG = -1e30


def rotate(vector, angles):
    half_dim = vector.shape[-1] // 2
    cosine = jnp.cos(angles)
    sine_part = jnp.sin(angles)
    leading = vector[..., :half_dim]
    trailing = vector[..., half_dim:]
    return jnp.concatenate(
        [leading * cosine - trailing * sine_part, trailing * cosine + leading * sine_part], axis=-1
    )


def rope_angles(lengths):
    half_dim = ROPE // 2
    inv_freq = THETA ** (-jnp.arange(half_dim, dtype=jnp.float32) * 2.0 / ROPE)
    return lengths.astype(jnp.float32)[:, None] * inv_freq[None, :]


def local(
    token_state,
    norm_gain,
    wq_nope,
    wq_rope,
    w_latent,
    w_rope_key,
    kv_gain,
    w_uk,
    w_uv,
    w_out,
    latent_cache,
    rope_cache,
    lengths,
):
    x_wide = token_state.astype(jnp.float32)
    scaled = (x_wide * norm_gain).astype(jnp.bfloat16)
    partials = (
        jnp.sum(x_wide * x_wide, axis=1),
        jnp.dot(scaled, wq_nope, preferred_element_type=jnp.float32),
        jnp.dot(scaled, wq_rope, preferred_element_type=jnp.float32),
        jnp.dot(scaled, w_latent, preferred_element_type=jnp.float32),
        jnp.dot(scaled, w_rope_key, preferred_element_type=jnp.float32),
    )
    squares, nope_sum, rope_sum, latent_sum, key_sum = lax.psum(
        (partials[0], partials[1], partials[2], partials[3], partials[4]), "kv"
    )
    inv_rms = lax.rsqrt(squares / D + EPS)[:, None]
    seq_count = token_state.shape[0]
    head_count = wq_nope.shape[1] // NOPE
    latent_raw = latent_sum * inv_rms
    latent_new = (
        latent_raw
        * lax.rsqrt(jnp.mean(latent_raw * latent_raw, axis=1, keepdims=True) + EPS)
        * kv_gain
    ).astype(jnp.bfloat16)
    angles = rope_angles(lengths)
    rope_new = rotate(key_sum * inv_rms, angles).astype(jnp.bfloat16)
    q_rot = rotate(
        (rope_sum * inv_rms).reshape(seq_count, head_count, ROPE), angles[:, None, :]
    ).astype(jnp.bfloat16)
    q_low = (nope_sum * inv_rms).astype(jnp.bfloat16).reshape(seq_count, head_count, NOPE)
    row_count = w_uk.shape[0]
    q_piece = jnp.einsum(
        "bhn,rhn->bhr",
        q_low,
        w_uk.reshape(row_count, head_count, NOPE),
        preferred_element_type=jnp.float32,
    ).astype(jnp.bfloat16)
    q_latent = lax.all_gather(q_piece, "kv", axis=2, tiled=True)
    block_len = latent_cache.shape[1]
    positions = lax.axis_index("kv") * block_len + jnp.arange(block_len, dtype=jnp.int32)
    score_scale = (NOPE + ROPE) ** (-0.5)
    cached = jnp.einsum("bhr,bpr->bhp", q_latent, latent_cache, preferred_element_type=jnp.float32)
    cached = cached + jnp.einsum(
        "bhk,bkp->bhp", q_rot, rope_cache, preferred_element_type=jnp.float32
    )
    own = jnp.einsum("bhr,br->bh", q_latent, latent_new, preferred_element_type=jnp.float32)
    own = own + jnp.einsum("bhk,bk->bh", q_rot, rope_new, preferred_element_type=jnp.float32)
    limit = lengths[:, None, None]
    newslot = positions[None, None, :] == limit
    usable = (positions[None, None, :] < limit) | newslot
    scores = jnp.where(newslot, own[:, :, None], cached) * score_scale
    masked = jnp.where(usable, scores, NEG)
    local_max = jnp.max(masked, axis=2)
    weights = jnp.where(usable, jnp.exp(masked - local_max[..., None]), 0.0)
    totals = jnp.sum(weights, axis=2)
    rounded = weights.astype(jnp.bfloat16)
    cache_weights = jnp.where(newslot, jnp.zeros_like(rounded), rounded)
    weighted = jnp.einsum(
        "bhp,bpr->bhr", cache_weights, latent_cache, preferred_element_type=jnp.float32
    )
    own_low = lax.optimization_barrier(jnp.where(newslot, rounded, jnp.zeros_like(rounded)))
    own_weight = jnp.sum(own_low.astype(jnp.float32), axis=2)
    weighted = weighted + own_weight[..., None] * latent_new.astype(jnp.float32)[:, None, :]
    value_rows = w_uv.shape[0]
    w_values = w_uv.reshape(value_rows, head_count, V_DIM)
    highest = lax.pmax(local_max, "kv")
    factor = jnp.exp(local_max - highest)
    latent_piece = lax.psum_scatter(
        weighted * factor[..., None], "kv", scatter_dimension=2, tiled=True
    ).astype(jnp.bfloat16)
    partial_values = jnp.einsum(
        "bhr,rhv->bhv", latent_piece, w_values, preferred_element_type=jnp.float32
    )
    value_sum, totals = lax.psum((partial_values, totals * factor), "kv")
    values = value_sum / totals[:, :, None]
    attended = values.astype(jnp.bfloat16).reshape(seq_count, head_count * V_DIM)
    out_term = jnp.dot(attended, w_out, preferred_element_type=jnp.float32)
    mixed = lax.psum_scatter(out_term.astype(jnp.bfloat16), "tp", scatter_dimension=1, tiled=True)
    return (mixed, latent_new, rope_new)


def solution(mesh):
    return jax.shard_map(
        local,
        mesh=mesh,
        in_specs=(
            P("dp", "kv"),
            P("kv"),
            P("kv", "tp"),
            P("kv", "tp"),
            P("kv", None),
            P("kv", None),
            P(),
            P("kv", "tp"),
            P("kv", "tp"),
            P("tp", "kv"),
            P("dp", "kv", None),
            P("dp", None, "kv"),
            P("dp"),
        ),
        out_specs=(P("dp", ("kv", "tp")), P("dp", None), P("dp", None)),
        check_vma=False,
    )
```

profile of v0, /device:TPU:0, one launch (start us, length us, event | category | flops | bytes accessed | tf_op | source)
XLA Modules:
  0.0 136.6 jit_solution(9274433471304251241)
XLA Ops:
  7.2 0.0 copy-start
  7.2 0.0 copy-start.2
  7.2 0.0 copy-start.5
  7.2 0.0 all-reduce.4.cloned.1.call-start
  7.2 1.5 %fusion.12 = f32[16]{0:T(128)} fusion(bf16[16,1024]{1,0:T(8,128)(2,1)} %param.13), kind=kLoop, calls=%fused_computation.21 | loop fusion | flops 49136 | bytes 32832 | tf_op jit(solution)/shard_map/reduce_sum | solution.py:52
  8.8 1.6 %fusion.19 = f32[16,32]{1,0:T(8,128)} fusion(bf16[1024,32]{0,1:T(8,128)(2,1)} %param.18, bf16[16,1024]{1,0:T(8,128)(2,1)} %param.13, f32[1024]{0:T(1024)} %param.14), kind=kOutput, calls=%fused_computation.37 | convolution fusion | flops 1097728 | bytes 104448 | tf_op jit(solution)/shard_map/dot_general | solution.py:56
  10.4 1.9 %fusion.21 = f32[16,256]{1,0:T(8,128)} fusion(bf16[1024,256]{1,0:T(8,128)(2,1)} %param.16, bf16[16,1024]{1,0:T(8,128)(2,1)} %param.13, f32[1024]{0:T(1024)} %param.14), kind=kOutput, calls=%fused_computation.38 | convolution fusion | flops 8437760 | bytes 577536 | tf_op jit(solution)/shard_map/dot_general | solution.py:54
  12.3 2.1 %fusion.25 = f32[16,512]{1,0:T(8,128)} fusion(bf16[1024,512]{1,0:T(8,128)(2,1)} %param.15, bf16[16,1024]{1,0:T(8,128)(2,1)} %param.13, f32[1024]{0:T(1024)} %param.14), kind=kOutput, calls=%fused_computation.40 | convolution fusion | flops 16826368 | bytes 1118208 | tf_op jit(solution)/shard_map/dot_general | solution.py:53
  14.4 2.1 %fusion.23 = f32[16,512]{1,0:T(8,128)} fusion(bf16[1024,512]{1,0:T(8,128)(2,1)} %param.17, bf16[16,1024]{1,0:T(8,128)(2,1)} %param.13, f32[1024]{0:T(1024)} %param.14), kind=kOutput, calls=%fused_computation.39 | convolution fusion | flops 16826368 | bytes 1118208 | tf_op jit(solution)/shard_map/dot_general | solution.py:55
  16.5 0.0 all-reduce.4.cloned.1.call-update
  16.5 0.0 reduce-scatter.3.cloned.1.call-start
  16.6 0.7 convert_element_type.47
  17.2 0.7 broadcast_compare_fusion
  18.0 0.0 copy-done.2
  18.0 0.1 copy.29
  18.1 36.0 %all-reduce.4.cloned.1.call-done = (f32[16,512]{1,0:T(8,128)}, f32[16]{0:T(128)}, f32[16,512]{1,0:T(8,128)}, f32[16,32]{1,0:T(8,128)}, f32[16,256]{1,0:T(8,128)}) async-done(((f32[16,512]{1,0:T(8,128)}, f32[16]{0:T(128)}, f32[16,512]{1,0:T(8,128)}, f32[16,32]{1,0:T(8,128)}, f32[16,256]{1,0:T(8,128)}), (f32[16,512]{1,0:T(8,128)}, f32[16]{0:T(128)}, f32[16,512]{1,0:T(8,128)}, f32[16,32]{1,0:T(8,128)}, ...) | async-done | bytes 84048 | tf_op jit(solution)/shard_map/psum | solution.py:58
  54.1 0.7 add_rsqrt_fusion.1
  54.7 0.8 broadcast_multiply_fusion.1
  55.5 0.8 broadcast_multiply_fusion
  56.3 0.9 multiply_reduce_fusion
  57.2 0.0 copy-done.5
  57.3 0.9 fusion.35
  58.1 0.0 copy-start.4
  58.1 0.1 reshape.170
  58.2 0.1 reshape.172
  58.3 0.0 copy-start.1
  58.3 0.1 fusion.4
  58.4 12.4 %all_gather.3 = bf16[16,8,512]{2,0,1:T(8,128)(2,1)S(1)} all-gather(bf16[16,8,128]{2,0,1:T(8,128)(2,1)S(1)} %fusion.4), channel_id=1, replica_groups=mesh['dp'=4,'kv'=4,'tp'=2] {'kv'}, dimensions={2}, use_global_device_ids=true | all-gather | bytes 163840 | tf_op jit(solution)/shard_map/all_gather | solution.py:83
  70.8 0.2 fusion.5
  71.0 0.0 copy-done
  71.0 0.9 fusion.7
  71.9 0.0 copy-start.3
  71.9 0.1 multiply_cosine_fusion
  72.1 0.1 fusion.48
  72.2 0.1 subtract_convert_fusion
  72.3 0.2 fusion.27
  72.5 0.0 copy-done.1
  72.5 0.3 fusion.36
  72.8 9.7 %pmax.7 = f32[16,8]{1,0:T(8,128)S(1)} all-reduce(f32[16,8]{1,0:T(8,128)S(1)} %get-tuple-element.25), channel_id=1, replica_groups=mesh['dp'=4,'kv'=4,'tp'=2] {'kv'}, use_global_device_ids=true, to_apply=%region_9.10 | all-reduce | flops 128 | bytes 1024 | tf_op jit(solution)/shard_map/pmax | solution.py:111
  82.5 0.2 fusion.9
  82.7 0.1 broadcast_select_fusion
  82.8 0.1 convert_reduce_fusion
  82.9 1.3 fusion
  84.2 0.0 copy-done.4
  84.2 0.0 reduce-scatter.3.cloned.1.call-update
  84.2 0.0 reduce-scatter.5.cloned.1.call-start
  84.3 0.0 copy-done.3
  84.3 0.1 copy.32
  84.4 18.4 %reduce-scatter.3.cloned.1.call-done = f32[16,8,128]{2,1,0:T(8,128)} async-done(((f32[16,8,512]{2,1,0:T(8,128)}), f32[16,8,128]{2,1,0:T(8,128)}) %reduce-scatter.3.cloned.1.call-update) | async-done | bytes 65552 | tf_op jit(solution)/shard_map/reduce_scatter | solution.py:113
  102.8 0.8 convert_element_type.51
  103.6 0.2 convolution_bitcast_fusion
  103.8 17.2 %all-reduce = (f32[16,8,64]{2,0,1:T(8,128)S(1)}, f32[16,8]{1,0:T(8,128)S(1)}) all-reduce(f32[16,8,64]{2,0,1:T(8,128)S(1)} %convolution_bitcast_fusion, f32[16,8]{1,0:T(8,128)S(1)} %get-tuple-element.10), channel_id=1, replica_groups=mesh['dp'=4,'kv'=4,'tp'=2] {'kv'}, use_global_device_ids=true, to_apply=%region_11.12 | all-reduce | flops 8320 | bytes 66560 | tf_op jit(solution)/shard_map/psum | solution.py:119
  121.0 0.1 copy.34
  121.0 0.1 divide_convert_fusion
  121.1 0.1 reshape.174
  121.2 2.1 %convolution_convert_fusion = bf16[16,1024]{1,0:T(8,128)(2,1)} fusion(bf16[16,512]{1,0:T(8,128)(2,1)S(1)} %reshape.174, bf16[512,1024]{1,0:T(8,128)(2,1)} %param.22), kind=kOutput, calls=%fused_computation.7 | convolution fusion | flops 16793600 | bytes 1097728 | tf_op jit(solution)/shard_map/dot_general | solution.py:122
  123.3 0.0 reduce-scatter.5.cloned.1.call-update
  123.4 0.7 pad_maximum_fusion.3
  124.0 6.0 %reduce-scatter.5.cloned.1.call-done = bf16[16,512]{1,0:T(8,128)(2,1)} async-done(((bf16[16,1024]{1,0:T(8,128)(2,1)}), bf16[16,512]{1,0:T(8,128)(2,1)}) %reduce-scatter.5.cloned.1.call-update) | async-done | bytes 16400 | tf_op jit(solution)/shard_map/reduce_scatter | solution.py:123
  (6 shorter events, 0.0 us)
Async XLA Ops:
  7.2 63.9 %copy-start = (bf16[16,192,512]{2,1,0:T(8,128)(2,1)S(1)}, bf16[16,192,512]{2,1,0:T(8,128)(2,1)}, u32[]{:S(2)}) copy-start(bf16[16,192,512]{2,1,0:T(8,128)(2,1)} %param.23) | copy-start | bytes 9437188
  7.2 10.8 %copy-start.2 = (bf16[128,512]{1,0:T(8,128)(2,1)S(1)}, bf16[128,512]{1,0:T(8,128)(2,1)}, u32[]{:S(2)}) copy-start(bf16[128,512]{1,0:T(8,128)(2,1)} %param.20) | copy-start | bytes 393220
  7.2 50.1 %copy-start.5 = (f32[512]{0:T(512)S(1)}, f32[512]{0:T(512)}, u32[]{:S(2)}) copy-start(f32[512]{0:T(512)} %param.19) | copy-start | bytes 6148
  7.2 46.9 %all-reduce.4.cloned.1.call-start = ((), (), s32[]{:S(2)}) async-start(), calls=%async_computation.4 | async-start | bytes 181248 | tf_op jit(solution)/shard_map/psum | solution.py:58
  16.5 86.3 %reduce-scatter.3.cloned.1.call-start = ((), (), s32[]{:S(2)}) async-start(), calls=%async_computation.2 | async-start | bytes 327680 | tf_op jit(solution)/shard_map/reduce_scatter | solution.py:113
  58.1 26.1 %copy-start.4 = (bf16[16,512]{1,0:T(8,128)(2,1)}, bf16[16,512]{1,0:T(8,128)(2,1)S(1)}, u32[]{:S(2)}) copy-start(bf16[16,512]{1,0:T(8,128)(2,1)S(1)} %get-tuple-element.13) | copy-start | bytes 49156
  58.3 14.2 %copy-start.1 = (bf16[16,32,192]{2,1,0:T(8,128)(2,1)S(1)}, bf16[16,32,192]{2,1,0:T(8,128)(2,1)}, u32[]{:S(2)}) copy-start(bf16[16,32,192]{2,1,0:T(8,128)(2,1)} %param.24) | copy-start | bytes 589828
  71.9 12.4 %copy-start.3 = (bf16[128,512]{1,0:T(8,128)(2,1)S(1)}, bf16[128,512]{1,0:T(8,128)(2,1)}, u32[]{:S(2)}) copy-start(bf16[128,512]{1,0:T(8,128)(2,1)} %param.21) | copy-start | bytes 393220
  84.2 45.8 %reduce-scatter.5.cloned.1.call-start = ((), (), s32[]{:S(2)}) async-start(), calls=%async_computation.3 | async-start | bytes 49152 | tf_op jit(solution)/shard_map/reduce_scatter | solution.py:123
Sparse Core Ops, SparseCore 0:
  16.6 37.3 all-reduce.3
  84.4 18.3 reduce-scatter.2
  123.5 6.5 reduce-scatter.4
where the time goes:
time: 137 us
  waiting for transfers between devices  60.4 us (44%)
  blocking collectives  39.3 us (29%)
  between operations  13.9 us (10%)
  matrix products  13 us (9%)
  other arithmetic  9.26 us (7%)
    psum x1, waiting for transfers between devices, local(): lax.psum((partials[0], partials[1], partials[2], partials[3], partials[4]...  36 us
    reduce_scatter x1, waiting for transfers between devices, local(): lax.psum_scatter(weighted * factor[..., None], 'kv', scatter_dimension=2,...  18.4 us
    psum x1, blocking collectives, local(): value_sum, totals = lax.psum((partial_values, totals * factor), 'kv')  17.2 us
    all_gather x1, blocking collectives, local(): q_latent = lax.all_gather(q_piece, 'kv', axis=2, tiled=True)  12.4 us
    pmax x1, blocking collectives, local(): highest = lax.pmax(local_max, 'kv')  9.74 us
    reduce_scatter x1, waiting for transfers between devices, local(): lax.psum_scatter(out_term.astype(jnp.bfloat16), 'tp', scatter_dimension=1...  6 us
  transfers between devices with their start and end apart: 3, of which 3 were waited for; matrix products, arithmetic and copies ran while one was open for 2% of the time, Pallas kernels for 0%

commit v1 on v0

--- a/solution.py
+++ b/solution.py
@@ -1,6 +1,11 @@
+import functools
+
 import jax
 import jax.numpy as jnp
+import numpy as np
 from jax import lax
+from jax.experimental import pallas as pl
+from jax.experimental.pallas import tpu as pltpu
 from jax.sharding import PartitionSpec as P
 
 D = 4096
@@ -12,6 +17,10 @@
 EPS = 1e-06
 THETA = 10000.0
 NEG = -1e30
+LANES = 128
+MESH = pl.DeviceIdType.MESH
+BF16 = jnp.bfloat16
+F32 = jnp.float32
 
 
 def rotate(vector, angles):
@@ -29,6 +38,371 @@
     half_dim = ROPE // 2
     inv_freq = THETA ** (-jnp.arange(half_dim, dtype=jnp.float32) * 2.0 / ROPE)
     return lengths.astype(jnp.float32)[:, None] * inv_freq[None, :]
+
+
+def dot_nt(a, b):
+    return lax.dot_general(a, b, (((1,), (1,)), ((), ())), preferred_element_type=F32)
+
+
+def dot(a, b):
+    return jnp.dot(a, b, preferred_element_type=F32)
+
+
+def swap_halves(u):
+    width = u.shape[1]
+    half = ROPE // 2
+    lane = lax.broadcasted_iota(jnp.int32, u.shape, 1)
+    from_above = pltpu.roll(u, width - half, 1)
+    from_below = pltpu.roll(u, half, 1)
+    return jnp.where(lane % ROPE < half, -from_above, from_below)
+
+
+def per_head(u, heads, width):
+    seqs, cols = u.shape
+    wide = jnp.broadcast_to(u[:, None, :], (seqs, heads, cols))
+    head = lax.broadcasted_iota(jnp.int32, wide.shape, 1)
+    lane = lax.broadcasted_iota(jnp.int32, wide.shape, 2)
+    return jnp.where(lane // width == head, wide, 0.0).reshape(seqs * heads, cols)
+
+
+def kernel(
+    n_kv,
+    n_tp,
+    len_ref,
+    freq_ref,
+    x_hbm,
+    gain_hbm,
+    wqn_hbm,
+    wqr_hbm,
+    wl_hbm,
+    wk_hbm,
+    kvg_hbm,
+    wuk_hbm,
+    wuv_hbm,
+    wo_hbm,
+    cache_hbm,
+    rope_hbm,
+    mixed_ref,
+    lnew_ref,
+    rnew_ref,
+    x,
+    gain,
+    wqn,
+    wqr,
+    wl,
+    wk,
+    kvg,
+    wuk,
+    wuv,
+    wo,
+    cache,
+    rope,
+    part_q,
+    part_l,
+    part_v,
+    half_out,
+    half_in,
+    scores,
+    load_sem,
+    send_sem,
+    recv_sem,
+    tp_sem,
+):
+    me = lax.axis_index("kv")
+    core = lax.axis_index("tp")
+    seqs = x.shape[0]
+    heads = wqn.shape[1] // NOPE
+    rank = wl.shape[1]
+    nope_cols = wqn.shape[1]
+    rope_cols = wqr.shape[1]
+    block = cache.shape[1]
+    rows = wuk_hbm.shape[0]
+
+    pairs = (
+        (x_hbm, x),
+        (gain_hbm, gain),
+        (wqn_hbm, wqn),
+        (wqr_hbm, wqr),
+        (wk_hbm, wk),
+        (wl_hbm, wl),
+        (kvg_hbm, kvg),
+        (wuk_hbm, wuk.at[me]),
+        (rope_hbm, rope),
+        (cache_hbm, cache),
+        (wuv_hbm, wuv.at[me]),
+        (wo_hbm, wo),
+    )
+    loads = [pltpu.make_async_copy(s, d, load_sem.at[i]) for i, (s, d) in enumerate(pairs)]
+    for load in loads:
+        load.start()
+
+    barrier = pltpu.get_barrier_semaphore()
+    for j in range(1, n_kv):
+        pl.semaphore_signal(
+            barrier, inc=1, device_id={"kv": lax.rem(me + j, n_kv)}, device_id_type=MESH
+        )
+    for j in range(1, n_tp):
+        pl.semaphore_signal(
+            barrier, inc=1, device_id={"tp": lax.rem(core + j, n_tp)}, device_id_type=MESH
+        )
+    pl.semaphore_wait(barrier, n_kv - 1 + n_tp - 1)
+
+    def copies(phase, src, dst):
+        return [
+            pltpu.make_async_remote_copy(
+                src_ref=src,
+                dst_ref=dst.at[me],
+                send_sem=send_sem.at[phase, j - 1],
+                recv_sem=recv_sem.at[phase, me],
+                device_id={"kv": lax.rem(me + j, n_kv)},
+                device_id_type=MESH,
+            )
+            for j in range(1, n_kv)
+        ]
+
+    def arrive(phase, dst):
+        for j in range(1, n_kv):
+            source = lax.rem(me + j, n_kv)
+            pltpu.make_async_remote_copy(
+                src_ref=dst.at[source],
+                dst_ref=dst.at[source],
+                send_sem=send_sem.at[phase, j - 1],
+                recv_sem=recv_sem.at[phase, source],
+                device_id={"kv": source},
+                device_id_type=MESH,
+            ).wait_recv()
+
+    sent = []
+
+    def send(phase, src, dst):
+        group = copies(phase, src, dst)
+        for c in group:
+            c.start()
+        sent.extend(group)
+
+    send(0, wuk_hbm, wuk)
+
+    loads[0].wait()
+    loads[1].wait()
+    x_wide = x[...].astype(F32)
+    scaled = (x_wide * gain[...]).astype(BF16)
+    squares = jnp.sum(x_wide * x_wide, axis=1, keepdims=True)
+    loads[2].wait()
+    part_q[me, :, :nope_cols] = dot(scaled, wqn[...])
+    loads[3].wait()
+    part_q[me, :, nope_cols : nope_cols + rope_cols] = dot(scaled, wqr[...])
+    loads[4].wait()
+    tail = slice(nope_cols + rope_cols, nope_cols + rope_cols + LANES)
+    part_q[me, :, tail] = jnp.broadcast_to(squares, (seqs, LANES))
+    part_q[me, :, nope_cols + rope_cols : nope_cols + rope_cols + ROPE] = dot(scaled, wk[...])
+    send(1, part_q.at[me], part_q)
+    loads[5].wait()
+    part_l[me] = dot(scaled, wl[...])
+    send(2, part_l.at[me], part_l)
+    send(3, wuv_hbm, wuv)
+
+    row = lax.broadcasted_iota(jnp.int32, (seqs, rope_cols), 0)
+    length_rows = jnp.zeros((seqs, rope_cols), jnp.int32)
+    for b in range(seqs):
+        length_rows = jnp.where(row == b, len_ref[b], length_rows)
+    angles = length_rows.astype(F32) * freq_ref[...]
+    cosine = jnp.cos(angles)
+    sine = jnp.sin(angles)
+
+    arrive(1, part_q)
+    total_q = part_q[0]
+    for s in range(1, n_kv):
+        total_q = total_q + part_q[s]
+    last = total_q[:, tail]
+    inv_rms = lax.rsqrt(last[:, ROPE : ROPE + 1] / D + EPS)
+    q_low = (total_q[:, :nope_cols] * inv_rms).astype(BF16).astype(F32)
+    q_rope = total_q[:, nope_cols : nope_cols + rope_cols] * inv_rms
+    q_rot = (q_rope * cosine + swap_halves(q_rope) * sine).astype(BF16).astype(F32)
+    key_raw = last * inv_rms
+    rope_new = key_raw * cosine[:, :LANES] + swap_halves(key_raw) * sine[:, :LANES]
+    rope_new = rope_new.astype(BF16)
+    rnew_ref[...] = rope_new[:, :ROPE]
+
+    q_blocks = per_head(q_low, heads, NOPE).astype(BF16)
+    r_blocks = per_head(q_rot, heads, ROPE).astype(BF16)
+    pick = (
+        lax.broadcasted_iota(jnp.int32, (rope_cols, LANES), 0) % ROPE
+        == lax.broadcasted_iota(jnp.int32, (rope_cols, LANES), 1)
+    )
+    q_rot_rows = dot(r_blocks, jnp.where(pick, 1.0, 0.0).astype(BF16))
+
+    loads[7].wait()
+    arrive(0, wuk)
+    q_latent = jnp.concatenate(
+        [dot_nt(q_blocks, wuk[s]) for s in range(n_kv)], axis=1
+    ).astype(BF16).astype(F32)
+
+    loads[8].wait()
+    loads[9].wait()
+    for b in range(seqs):
+        at = slice(b * heads, (b + 1) * heads)
+        scores[at, :] = dot_nt(q_latent[at].astype(BF16), cache[b]) + dot(
+            q_rot_rows[at, :ROPE].astype(BF16), rope[b]
+        )
+
+    loads[6].wait()
+    arrive(2, part_l)
+    total_l = part_l[0]
+    for s in range(1, n_kv):
+        total_l = total_l + part_l[s]
+    latent_raw = total_l * inv_rms
+    mean_square = jnp.mean(latent_raw * latent_raw, axis=1, keepdims=True)
+    latent_new = (latent_raw * lax.rsqrt(mean_square + EPS) * kvg[...]).astype(BF16)
+    lnew_ref[...] = latent_new
+
+    def rows_of(u):
+        return jnp.broadcast_to(u[:, None, :], (seqs, heads, u.shape[1])).reshape(
+            seqs * heads, u.shape[1]
+        )
+
+    new_rows = rows_of(latent_new.astype(F32))
+    key_rows = rows_of(rope_new.astype(F32))
+    own = jnp.sum(q_latent * new_rows, axis=1, keepdims=True)
+    own = own + jnp.sum(q_rot_rows * key_rows, axis=1, keepdims=True)
+
+    score_scale = (NOPE + ROPE) ** (-0.5)
+    limit = jnp.concatenate(
+        [jnp.full((heads, block), len_ref[b], jnp.int32) for b in range(seqs)], axis=0
+    )
+    place = me * block + lax.broadcasted_iota(jnp.int32, (seqs * heads, block), 1)
+    newslot = place == limit
+    usable = place <= limit
+    masked = jnp.where(usable, jnp.where(newslot, own, scores[...]) * score_scale, NEG)
+    local_max = jnp.max(masked, axis=1, keepdims=True)
+    weights = jnp.where(usable, jnp.exp(masked - local_max), 0.0)
+    totals = jnp.sum(weights, axis=1, keepdims=True)
+    rounded = weights.astype(BF16).astype(F32)
+    own_weight = jnp.sum(jnp.where(newslot, rounded, 0.0), axis=1, keepdims=True)
+    cache_weights = jnp.where(newslot, 0.0, rounded)
+    weighted = jnp.concatenate(
+        [
+            dot(cache_weights[b * heads : (b + 1) * heads].astype(BF16), cache[b])
+            for b in range(seqs)
+        ],
+        axis=0,
+    )
+    weighted = (weighted + own_weight * new_rows).astype(BF16)
+
+    loads[10].wait()
+    arrive(3, wuv)
+    values = dot(weighted[:, :rows], wuv[0])
+    for s in range(1, n_kv):
+        values = values + dot(weighted[:, s * rows : (s + 1) * rows], wuv[s])
+    cols = values.shape[1]
+    values = values.reshape(seqs, heads, cols)
+    head = lax.broadcasted_iota(jnp.int32, values.shape, 1)
+    lane = lax.broadcasted_iota(jnp.int32, values.shape, 2)
+    part_v[me, :, :cols] = jnp.sum(jnp.where(lane // V_DIM == head, values, 0.0), axis=1)
+    shape = (seqs, heads, LANES)
+    head = lax.broadcasted_iota(jnp.int32, shape, 1)
+    lane = lax.broadcasted_iota(jnp.int32, shape, 2)
+    stats = jnp.where(
+        lane == head, jnp.broadcast_to(local_max, (seqs * heads, LANES)).reshape(shape), 0.0
+    ) + jnp.where(
+        lane == head + LANES // 2,
+        jnp.broadcast_to(totals, (seqs * heads, LANES)).reshape(shape),
+        0.0,
+    )
+    part_v[me, :, cols:] = jnp.sum(stats, axis=1)
+    send(4, part_v.at[me], part_v)
+    arrive(4, part_v)
+
+    maxima = [part_v[s, :, cols:] for s in range(n_kv)]
+    sums = [pltpu.roll(m, LANES // 2, 1) for m in maxima]
+    highest = functools.reduce(jnp.maximum, maxima)
+    factors = [jnp.exp(m - highest) for m in maxima]
+    whole = functools.reduce(jnp.add, [f * t for f, t in zip(factors, sums)])
+    lane = lax.broadcasted_iota(jnp.int32, (seqs, cols), 1)
+
+    def spread(u):
+        out = jnp.broadcast_to(u[:, :1], (seqs, cols))
+        for h in range(1, heads):
+            out = jnp.where(lane // V_DIM == h, u[:, h : h + 1], out)
+        return out
+
+    merged = part_v[0, :, :cols] * spread(factors[0])
+    for s in range(1, n_kv):
+        merged = merged + part_v[s, :, :cols] * spread(factors[s])
+    attended = (merged / spread(whole)).astype(BF16)
+
+    loads[11].wait()
+    width = half_in.shape[1]
+    other = lax.rem(core + 1, n_tp)
+    half_out[...] = dot(attended, wo[:, pl.ds(pl.multiple_of(other * width, width), width)]).astype(
+        BF16
+    )
+    swap = pltpu.make_async_remote_copy(
+        src_ref=half_out,
+        dst_ref=half_in,
+        send_sem=tp_sem.at[0],
+        recv_sem=tp_sem.at[1],
+        device_id={"tp": other},
+        device_id_type=MESH,
+    )
+    swap.start()
+    mine = dot(attended, wo[:, pl.ds(pl.multiple_of(core * width, width), width)]).astype(BF16)
+    swap.wait()
+    mixed_ref[...] = (mine.astype(F32) + half_in[...].astype(F32)).astype(BF16)
+    for c in sent:
+        c.wait_send()
+
+
+def fused(n_kv, n_tp, *args):
+    (x, gain, wqn, wqr, wl, wk, kvg, wuk, wuv, wo, cache, rope, lengths) = args
+    seqs, rank = x.shape[0], wl.shape[1]
+    heads = wqn.shape[1] // NOPE
+    q_cols = wqn.shape[1] + wqr.shape[1] + LANES
+    half = wo.shape[1] // n_tp
+    freq = THETA ** (-(np.arange(wqr.shape[1]) % (ROPE // 2)) * 2.0 / ROPE)
+    freq = jnp.asarray(freq.astype(np.float32)[None, :])
+    any_spec = pl.BlockSpec(memory_space=pl.ANY)
+    vmem = pl.BlockSpec(memory_space=pltpu.VMEM)
+
+    def like(a, *lead):
+        return pltpu.VMEM(tuple(lead) + a.shape, a.dtype)
+
+    gain = gain.reshape(1, -1)
+    kvg = kvg.reshape(1, -1)
+    return pl.pallas_call(
+        functools.partial(kernel, n_kv, n_tp),
+        out_shape=(
+            jax.ShapeDtypeStruct((seqs, half), BF16),
+            jax.ShapeDtypeStruct((seqs, rank), BF16),
+            jax.ShapeDtypeStruct((seqs, ROPE), BF16),
+        ),
+        in_specs=[pl.BlockSpec(memory_space=pltpu.SMEM), vmem] + [any_spec] * 12,
+        out_specs=(vmem, vmem, vmem),
+        scratch_shapes=[
+            like(x),
+            like(gain),
+            like(wqn),
+            like(wqr),
+            like(wl),
+            like(wk),
+            like(kvg),
+            like(wuk, n_kv),
+            like(wuv, n_kv),
+            like(wo),
+            like(cache),
+            like(rope),
+            pltpu.VMEM((n_kv, seqs, q_cols), F32),
+            pltpu.VMEM((n_kv, seqs, rank), F32),
+            pltpu.VMEM((n_kv, seqs, wuv.shape[1] + LANES), F32),
+            pltpu.VMEM((seqs, half), BF16),
+            pltpu.VMEM((seqs, half), BF16),
+            pltpu.VMEM((seqs * heads, cache.shape[1]), F32),
+            pltpu.SemaphoreType.DMA((12,)),
+            pltpu.SemaphoreType.DMA((5, n_kv - 1)),
+            pltpu.SemaphoreType.DMA((5, n_kv)),
+            pltpu.SemaphoreType.DMA((2,)),
+        ],
+        compiler_params=pltpu.CompilerParams(collective_id=0, has_side_effects=True),
+    )(lengths, freq, x, gain, wqn, wqr, wl, wk, kvg, wuk, wuv, wo, cache, rope)
 
 
 def local(
@@ -125,8 +499,16 @@
 
 
 def solution(mesh):
+    n_kv, n_tp = mesh.shape["kv"], mesh.shape["tp"]
+
+    def body(*args):
+        width, rank = args[9].shape[1], args[4].shape[1]
+        if (width // n_tp) % LANES == 0 and (rank // n_kv) % LANES == 0:
+            return fused(n_kv, n_tp, *args)
+        return local(*args)
+
     return jax.shard_map(
-        local,
+        body,
         mesh=mesh,
         in_specs=(
             P("dp", "kv"),

time: 137 us -> 51 us (0.37)
  waiting for transfers between devices: 60.4 us -> 0 us
  Pallas kernels: 0 us -> 44.4 us
  blocking collectives: 39.3 us -> 0 us
  between operations: 13.9 us -> 0.64 us
  matrix products: 13 us -> 0 us
  other arithmetic: 9.26 us -> 0 us
  local copies, waits for them, and re-layouts: 0.61 us -> 5.59 us
    pallas_call x0 -> x1, Pallas kernels: none -> 44.4 us  [fused(): pl.pallas_call(functools.partial(kernel, n_kv, n_tp), out_shape=(jax.Shap...]
    psum x1 -> x0, waiting for transfers between devices: 36 us -> none  [local(): lax.psum((partials[0], partials[1], partials[2], partials[3], partials[4]...]
    reduce_scatter x2 -> x0, waiting for transfers between devices: 24.4 us -> none  [the longest x1 18.4 us: local(): lax.psum_scatter(weighted * factor[..., None], 'kv', scatter_dimension=2,...]
    psum x1 -> x0, blocking collectives: 17.2 us -> none  [local(): value_sum, totals = lax.psum((partial_values, totals * factor), 'kv')]
    dot_general x12 -> x0, matrix products: 13 us -> none  [the longest x1 2.11 us: local(): jnp.dot(scaled, w_latent, preferred_element_type=jnp.float32)]
    all_gather x1 -> x0, blocking collectives: 12.4 us -> none  [local(): q_latent = lax.all_gather(q_piece, 'kv', axis=2, tiled=True)]
    pmax x1 -> x0, blocking collectives: 9.74 us -> none  [local(): highest = lax.pmax(local_max, 'kv')]
    unnamed x14 -> x4, local copies, waits for them, and re-layouts: 0.27 us -> 5.59 us
  transfers between devices with their start and end apart: 3 -> 0, of which waited for: 3 -> 0; matrix products, arithmetic and copies ran while one was open for 2% -> 0% of each run, Pallas kernels for 0% -> 0%
where the time goes in v1:
time: 51 us; the launch traced here: 50.6 us
  Pallas kernels  44.4 us (87%)
  local copies, waits for them, and re-layouts  5.59 us (11%)
  between operations  0.64 us (1%)
    pallas_call x1, Pallas kernels, fused(): pl.pallas_call(functools.partial(kernel, n_kv, n_tp), out_shape=(jax.Shap...  44.4 us
    unnamed x4, local copies, waits for them, and re-layouts  5.59 us

profile of v1, /device:TPU:0, one launch (start us, length us, event | category | flops | bytes accessed | tf_op | source)
XLA Modules:
  0.0 50.6 jit_solution(11174457602428807267)
XLA Ops:
  0.6 1.7 %copy.17.wk_hbm = bf16[1024,32]{1,0:T(8,128)(2,1)} copy(bf16[1024,32]{0,1:T(8,128)(2,1)} %param.19) | data formatting | bytes 131072 | tf_op args[5]
  2.3 44.4 %shard_map.157 = (bf16[16,512]{1,0:T(8,128)(2,1)}, bf16[16,512]{1,0:T(8,128)(2,1)}, bf16[16,32]{1,0:T(8,128)(2,1)}) custom-call(s32[16]{0:T(128)} %len_ref.1, f32[1,256]{1,0:T(1,128)} %constant.2.clone.freq_ref, bf16[16,1024]{1,0:T(8,128)(2,1)} %x_hbm.1, f32[1,1024]{1,0:T(1,128)} %bitcast.2, bf16[1024,512]{1,0:T(8,128)(2,1)} %wqn_hbm.1, ...), custom_call_target="tpu_custom_call" | custom-call | tf_op jit(solution)/shard_map/pallas_call | solution.py:371
  46.7 1.3 %copy.21 = bf16[16,512]{1,0:T(8,128)(2,1)} copy(bf16[16,512]{1,0:T(8,128)(2,1)} %get-tuple-element.6) | data formatting | bytes 32768
  48.0 1.3 %copy.22 = bf16[16,512]{1,0:T(8,128)(2,1)} copy(bf16[16,512]{1,0:T(8,128)(2,1)} %get-tuple-element.7) | data formatting | bytes 32768
  49.3 1.3 %copy.23 = bf16[16,32]{1,0:T(8,128)(2,1)} copy(bf16[16,32]{1,0:T(8,128)(2,1)} %get-tuple-element.8) | data formatting | bytes 2048

commit v2 on v1

--- a/solution.py
+++ b/solution.py
@@ -57,15 +57,8 @@
     return jnp.where(lane % ROPE < half, -from_above, from_below)
 
 
-def per_head(u, heads, width):
-    seqs, cols = u.shape
-    wide = jnp.broadcast_to(u[:, None, :], (seqs, heads, cols))
-    head = lax.broadcasted_iota(jnp.int32, wide.shape, 1)
-    lane = lax.broadcasted_iota(jnp.int32, wide.shape, 2)
-    return jnp.where(lane // width == head, wide, 0.0).reshape(seqs * heads, cols)
-
-
 def kernel(
+    n_dp,
     n_kv,
     n_tp,
     len_ref,
@@ -97,36 +90,50 @@
     wo,
     cache,
     rope,
-    part_q,
-    part_l,
-    part_v,
+    key_pad,
+    q_out,
+    q_in,
+    lat_in,
+    lat_half,
+    q_lat,
+    q_rots,
+    val_in,
+    stat_in,
     half_out,
     half_in,
     scores,
     load_sem,
     send_sem,
     recv_sem,
+    dp_send,
+    dp_recv,
     tp_sem,
 ):
     me = lax.axis_index("kv")
     core = lax.axis_index("tp")
+    group = lax.axis_index("dp")
     seqs = x.shape[0]
     heads = wqn.shape[1] // NOPE
-    rank = wl.shape[1]
-    nope_cols = wqn.shape[1]
-    rope_cols = wqr.shape[1]
+    own_heads = heads // n_kv
+    rank = kvg.shape[1]
+    lat_cols = wl.shape[1]
     block = cache.shape[1]
-    rows = wuk_hbm.shape[0]
-
+    rows = wuv_hbm.shape[0]
+    part = rows // n_dp
+
+    def cols(index, width):
+        return pl.ds(pl.multiple_of(index * width, width), width)
+
+    part_rows = cols(group, part)
     pairs = (
         (x_hbm, x),
         (gain_hbm, gain),
         (wqn_hbm, wqn),
         (wqr_hbm, wqr),
         (wk_hbm, wk),
-        (wl_hbm, wl),
+        (wl_hbm.at[:, cols(core, lat_cols)], wl),
         (kvg_hbm, kvg),
-        (wuk_hbm, wuk.at[me]),
+        (wuk_hbm.at[:, cols(me, LANES)], wuk.at[me]),
         (rope_hbm, rope),
         (cache_hbm, cache),
         (wuv_hbm, wuv.at[me]),
@@ -137,131 +144,178 @@
         load.start()
 
     barrier = pltpu.get_barrier_semaphore()
-    for j in range(1, n_kv):
-        pl.semaphore_signal(
-            barrier, inc=1, device_id={"kv": lax.rem(me + j, n_kv)}, device_id_type=MESH
-        )
-    for j in range(1, n_tp):
-        pl.semaphore_signal(
-            barrier, inc=1, device_id={"tp": lax.rem(core + j, n_tp)}, device_id_type=MESH
-        )
-    pl.semaphore_wait(barrier, n_kv - 1 + n_tp - 1)
-
-    def copies(phase, src, dst):
-        return [
-            pltpu.make_async_remote_copy(
-                src_ref=src,
-                dst_ref=dst.at[me],
+    axes = (("kv", me, n_kv), ("tp", core, n_tp), ("dp", group, n_dp))
+    for name, index, size in axes:
+        for j in range(1, size):
+            pl.semaphore_signal(
+                barrier, inc=1, device_id={name: lax.rem(index + j, size)}, device_id_type=MESH
+            )
+    pl.semaphore_wait(barrier, n_kv - 1 + n_tp - 1 + n_dp - 1)
+
+    sent = []
+
+    def send(phase, src, dst):
+        for j in range(1, n_kv):
+            peer = lax.rem(me + j, n_kv)
+            copy = pltpu.make_async_remote_copy(
+                src_ref=src(peer),
+                dst_ref=dst(me),
                 send_sem=send_sem.at[phase, j - 1],
                 recv_sem=recv_sem.at[phase, me],
-                device_id={"kv": lax.rem(me + j, n_kv)},
+                device_id={"kv": peer},
                 device_id_type=MESH,
             )
-            for j in range(1, n_kv)
-        ]
+            copy.start()
+            sent.append(copy)
 
     def arrive(phase, dst):
         for j in range(1, n_kv):
             source = lax.rem(me + j, n_kv)
             pltpu.make_async_remote_copy(
-                src_ref=dst.at[source],
-                dst_ref=dst.at[source],
+                src_ref=dst(source),
+                dst_ref=dst(source),
                 send_sem=send_sem.at[phase, j - 1],
                 recv_sem=recv_sem.at[phase, source],
                 device_id={"kv": source},
                 device_id_type=MESH,
             ).wait_recv()
 
-    sent = []
-
-    def send(phase, src, dst):
-        group = copies(phase, src, dst)
-        for c in group:
-            c.start()
-        sent.extend(group)
-
-    send(0, wuk_hbm, wuk)
+    send(0, lambda p: wuk_hbm.at[:, cols(p, LANES)], lambda s: wuk.at[s])
 
     loads[0].wait()
     loads[1].wait()
     x_wide = x[...].astype(F32)
     scaled = (x_wide * gain[...]).astype(BF16)
     squares = jnp.sum(x_wide * x_wide, axis=1, keepdims=True)
+    key_pad[...] = jnp.broadcast_to(squares, key_pad.shape)
+    loads[4].wait()
+    key_pad[:, :ROPE] = dot_nt(scaled, wk[...])
+    rope_own = own_heads * ROPE
+    key_part = pltpu.roll(key_pad[...], rope_own, 1)
     loads[2].wait()
-    part_q[me, :, :nope_cols] = dot(scaled, wqn[...])
+    nope_part = dot(scaled, wqn[...])
     loads[3].wait()
-    part_q[me, :, nope_cols : nope_cols + rope_cols] = dot(scaled, wqr[...])
-    loads[4].wait()
-    tail = slice(nope_cols + rope_cols, nope_cols + rope_cols + LANES)
-    part_q[me, :, tail] = jnp.broadcast_to(squares, (seqs, LANES))
-    part_q[me, :, nope_cols + rope_cols : nope_cols + rope_cols + ROPE] = dot(scaled, wk[...])
-    send(1, part_q.at[me], part_q)
+    rope_part = dot(scaled, wqr[...])
+    lane = lax.broadcasted_iota(jnp.int32, (seqs, LANES), 1)
+    for s in range(n_kv):
+        q_out[s, :, :LANES] = nope_part[:, s * LANES : (s + 1) * LANES]
+        first, shift = divmod(s * rope_own, LANES)
+        piece = rope_part[:, first * LANES : (first + 1) * LANES]
+        if shift:
+            piece = pltpu.roll(piece, LANES - shift, 1)
+        q_out[s, :, LANES:] = jnp.where(lane < rope_own, piece, key_part)
+    send(1, lambda p: q_out.at[p], lambda s: q_in.at[s])
+    q_in[me] = q_out[me]
+    send(2, lambda p: wuv_hbm.at[part_rows], lambda s: wuv.at[s, part_rows])
     loads[5].wait()
-    part_l[me] = dot(scaled, wl[...])
-    send(2, part_l.at[me], part_l)
-    send(3, wuv_hbm, wuv)
-
-    row = lax.broadcasted_iota(jnp.int32, (seqs, rope_cols), 0)
-    length_rows = jnp.zeros((seqs, rope_cols), jnp.int32)
+    lat_in[me] = dot(scaled, wl[...])
+    send(3, lambda p: lat_in.at[me], lambda s: lat_in.at[s])
+
+    row = lax.broadcasted_iota(jnp.int32, (seqs, LANES), 0)
+    length_rows = jnp.zeros((seqs, LANES), jnp.int32)
     for b in range(seqs):
         length_rows = jnp.where(row == b, len_ref[b], length_rows)
     angles = length_rows.astype(F32) * freq_ref[...]
     cosine = jnp.cos(angles)
     sine = jnp.sin(angles)
 
-    arrive(1, part_q)
-    total_q = part_q[0]
+    arrive(1, lambda s: q_in.at[s])
+    total_q = q_in[0]
     for s in range(1, n_kv):
-        total_q = total_q + part_q[s]
-    last = total_q[:, tail]
-    inv_rms = lax.rsqrt(last[:, ROPE : ROPE + 1] / D + EPS)
-    q_low = (total_q[:, :nope_cols] * inv_rms).astype(BF16).astype(F32)
-    q_rope = total_q[:, nope_cols : nope_cols + rope_cols] * inv_rms
-    q_rot = (q_rope * cosine + swap_halves(q_rope) * sine).astype(BF16).astype(F32)
-    key_raw = last * inv_rms
-    rope_new = key_raw * cosine[:, :LANES] + swap_halves(key_raw) * sine[:, :LANES]
-    rope_new = rope_new.astype(BF16)
-    rnew_ref[...] = rope_new[:, :ROPE]
-
-    q_blocks = per_head(q_low, heads, NOPE).astype(BF16)
-    r_blocks = per_head(q_rot, heads, ROPE).astype(BF16)
+        total_q = total_q + q_in[s]
+    last = total_q[:, LANES:]
+    inv_rms = lax.rsqrt(last[:, LANES - 1 :] / D + EPS)
+    q_low = total_q[:, :LANES] * inv_rms
+    last = last * inv_rms
+    turned = (last * cosine + swap_halves(last) * sine).astype(BF16)
+    q_rots[me] = turned
+    send(4, lambda p: q_rots.at[me], lambda s: q_rots.at[s])
+    q_blocks = jnp.concatenate(
+        [jnp.where(lane // NOPE == h, q_low, 0.0) for h in range(own_heads)], axis=0
+    ).astype(BF16)
+    loads[7].wait()
+    arrive(0, lambda s: wuk.at[s])
+    for s in range(n_kv):
+        q_lat[me, :, s * rows : (s + 1) * rows] = dot_nt(q_blocks, wuk[s]).astype(BF16)
+    send(5, lambda p: q_lat.at[me], lambda s: q_lat.at[s])
+    rope_new = pltpu.roll(turned.astype(F32), LANES - rope_own, 1)
+    rnew_ref[...] = rope_new[:, :ROPE].astype(BF16)
+
+    arrive(2, lambda s: wuv.at[s, part_rows])
+    for j in range(1, n_dp):
+        peer = lax.rem(group + j, n_dp)
+        for i in range(1, n_kv):
+            source = lax.rem(me + i, n_kv)
+            copy = pltpu.make_async_remote_copy(
+                src_ref=wuv.at[source, part_rows],
+                dst_ref=wuv.at[source, part_rows],
+                send_sem=dp_send.at[j - 1, i - 1],
+                recv_sem=dp_recv.at[group, i - 1],
+                device_id={"dp": peer},
+                device_id_type=MESH,
+            )
+            copy.start()
+            sent.append(copy)
+
+    arrive(3, lambda s: lat_in.at[s])
+    total_l = lat_in[0]
+    for s in range(1, n_kv):
+        total_l = total_l + lat_in[s]
+    lat_half[core] = total_l
+    other = lax.rem(core + 1, n_tp)
+    lat_swap = pltpu.make_async_remote_copy(
+        src_ref=lat_half.at[core],
+        dst_ref=lat_half.at[core],
+        send_sem=tp_sem.at[0],
+        recv_sem=tp_sem.at[1],
+        device_id={"tp": other},
+        device_id_type=MESH,
+    )
+    lat_swap.start()
+
+    count = seqs * heads
+    to = lax.broadcasted_iota(jnp.int32, (count, count), 0)
+    frm = lax.broadcasted_iota(jnp.int32, (count, count), 1)
+    order = jnp.where(frm == (to % heads) * seqs + to // heads, 1.0, 0.0).astype(BF16)
+    arrive(4, lambda s: q_rots.at[s])
+    wide = jnp.concatenate([q_rots[s] for s in range(n_kv)], axis=1).astype(F32)
+    shape = (seqs, heads, n_kv * LANES)
+    head = lax.broadcasted_iota(jnp.int32, shape, 1)
+    at = lax.broadcasted_iota(jnp.int32, shape, 2)
+    mine = (at // LANES == head // own_heads) & ((at % LANES) // ROPE == head % own_heads)
+    r_blocks = jnp.where(mine, jnp.broadcast_to(wide[:, None, :], shape), 0.0)
+    r_blocks = r_blocks.reshape(count, n_kv * LANES).astype(BF16)
+    pick_shape = (n_kv * LANES, LANES)
     pick = (
-        lax.broadcasted_iota(jnp.int32, (rope_cols, LANES), 0) % ROPE
-        == lax.broadcasted_iota(jnp.int32, (rope_cols, LANES), 1)
+        lax.broadcasted_iota(jnp.int32, pick_shape, 0) % ROPE
+        == lax.broadcasted_iota(jnp.int32, pick_shape, 1)
     )
     q_rot_rows = dot(r_blocks, jnp.where(pick, 1.0, 0.0).astype(BF16))
-
-    loads[7].wait()
-    arrive(0, wuk)
-    q_latent = jnp.concatenate(
-        [dot_nt(q_blocks, wuk[s]) for s in range(n_kv)], axis=1
-    ).astype(BF16).astype(F32)
+    arrive(5, lambda s: q_lat.at[s])
+    q_latent = dot(order, q_lat[...].reshape(count, rank))
 
     loads[8].wait()
     loads[9].wait()
     for b in range(seqs):
-        at = slice(b * heads, (b + 1) * heads)
-        scores[at, :] = dot_nt(q_latent[at].astype(BF16), cache[b]) + dot(
-            q_rot_rows[at, :ROPE].astype(BF16), rope[b]
+        span = slice(b * heads, (b + 1) * heads)
+        scores[span, :] = dot_nt(q_latent[span].astype(BF16), cache[b]) + dot(
+            q_rot_rows[span, :ROPE].astype(BF16), rope[b]
         )
 
     loads[6].wait()
-    arrive(2, part_l)
-    total_l = part_l[0]
-    for s in range(1, n_kv):
-        total_l = total_l + part_l[s]
-    latent_raw = total_l * inv_rms
+    lat_swap.wait()
+    latent_raw = jnp.concatenate([lat_half[t] for t in range(n_tp)], axis=1) * inv_rms
     mean_square = jnp.mean(latent_raw * latent_raw, axis=1, keepdims=True)
     latent_new = (latent_raw * lax.rsqrt(mean_square + EPS) * kvg[...]).astype(BF16)
     lnew_ref[...] = latent_new
 
     def rows_of(u):
         return jnp.broadcast_to(u[:, None, :], (seqs, heads, u.shape[1])).reshape(
-            seqs * heads, u.shape[1]
+            count, u.shape[1]
         )
 
     new_rows = rows_of(latent_new.astype(F32))
-    key_rows = rows_of(rope_new.astype(F32))
+    key_rows = rows_of(rope_new)
     own = jnp.sum(q_latent * new_rows, axis=1, keepdims=True)
     own = own + jnp.sum(q_rot_rows * key_rows, axis=1, keepdims=True)
 
@@ -269,7 +323,7 @@
     limit = jnp.concatenate(
         [jnp.full((heads, block), len_ref[b], jnp.int32) for b in range(seqs)], axis=0
     )
-    place = me * block + lax.broadcasted_iota(jnp.int32, (seqs * heads, block), 1)
+    place = me * block + lax.broadcasted_iota(jnp.int32, (count, block), 1)
     newslot = place == limit
     usable = place <= limit
     masked = jnp.where(usable, jnp.where(newslot, own, scores[...]) * score_scale, NEG)
@@ -288,88 +342,97 @@
     )
     weighted = (weighted + own_weight * new_rows).astype(BF16)
 
-    loads[10].wait()
-    arrive(3, wuv)
-    values = dot(weighted[:, :rows], wuv[0])
-    for s in range(1, n_kv):
-        values = values + dot(weighted[:, s * rows : (s + 1) * rows], wuv[s])
-    cols = values.shape[1]
-    values = values.reshape(seqs, heads, cols)
-    head = lax.broadcasted_iota(jnp.int32, values.shape, 1)
-    lane = lax.broadcasted_iota(jnp.int32, values.shape, 2)
-    part_v[me, :, :cols] = jnp.sum(jnp.where(lane // V_DIM == head, values, 0.0), axis=1)
     shape = (seqs, heads, LANES)
     head = lax.broadcasted_iota(jnp.int32, shape, 1)
-    lane = lax.broadcasted_iota(jnp.int32, shape, 2)
+    at = lax.broadcasted_iota(jnp.int32, shape, 2)
     stats = jnp.where(
-        lane == head, jnp.broadcast_to(local_max, (seqs * heads, LANES)).reshape(shape), 0.0
+        at == head, jnp.broadcast_to(local_max, (count, LANES)).reshape(shape), 0.0
     ) + jnp.where(
-        lane == head + LANES // 2,
-        jnp.broadcast_to(totals, (seqs * heads, LANES)).reshape(shape),
-        0.0,
-    )
-    part_v[me, :, cols:] = jnp.sum(stats, axis=1)
-    send(4, part_v.at[me], part_v)
-    arrive(4, part_v)
-
-    maxima = [part_v[s, :, cols:] for s in range(n_kv)]
+        at == head + LANES // 2, jnp.broadcast_to(totals, (count, LANES)).reshape(shape), 0.0
+    )
+    stat_in[me] = jnp.sum(stats, axis=1)
+    send(6, lambda p: stat_in.at[me], lambda s: stat_in.at[s])
+    loads[10].wait()
+    for j in range(1, n_dp):
+        source_group = lax.rem(group + j, n_dp)
+        their_rows = cols(source_group, part)
+        for i in range(1, n_kv):
+            source = lax.rem(me + i, n_kv)
+            pltpu.make_async_remote_copy(
+                src_ref=wuv.at[source, their_rows],
+                dst_ref=wuv.at[source, their_rows],
+                send_sem=dp_send.at[j - 1, i - 1],
+                recv_sem=dp_recv.at[source_group, i - 1],
+                device_id={"dp": source_group},
+                device_id_type=MESH,
+            ).wait_recv()
+    values = dot(weighted, wuv[...].reshape(rank, wuv.shape[2]))
+    width = values.shape[1]
+    values = values.reshape(seqs, heads, width)
+    head = lax.broadcasted_iota(jnp.int32, values.shape, 1)
+    at = lax.broadcasted_iota(jnp.int32, values.shape, 2)
+    val_in[me] = jnp.sum(jnp.where(at // V_DIM == head, values, 0.0), axis=1).astype(BF16)
+    send(7, lambda p: val_in.at[me], lambda s: val_in.at[s])
+
+    arrive(6, lambda s: stat_in.at[s])
+    maxima = [stat_in[s] for s in range(n_kv)]
     sums = [pltpu.roll(m, LANES // 2, 1) for m in maxima]
     highest = functools.reduce(jnp.maximum, maxima)
     factors = [jnp.exp(m - highest) for m in maxima]
     whole = functools.reduce(jnp.add, [f * t for f, t in zip(factors, sums)])
-    lane = lax.broadcasted_iota(jnp.int32, (seqs, cols), 1)
+    at = lax.broadcasted_iota(jnp.int32, (seqs, width), 1)
 
     def spread(u):
-        out = jnp.broadcast_to(u[:, :1], (seqs, cols))
+        out = jnp.broadcast_to(u[:, :1], (seqs, width))
         for h in range(1, heads):
-            out = jnp.where(lane // V_DIM == h, u[:, h : h + 1], out)
+            out = jnp.where(at // V_DIM == h, u[:, h : h + 1], out)
         return out
 
-    merged = part_v[0, :, :cols] * spread(factors[0])
+    spreads = [spread(f) for f in factors]
+    divisor = spread(whole)
+    arrive(7, lambda s: val_in.at[s])
+    merged = val_in[0].astype(F32) * spreads[0]
     for s in range(1, n_kv):
-        merged = merged + part_v[s, :, :cols] * spread(factors[s])
-    attended = (merged / spread(whole)).astype(BF16)
+        merged = merged + val_in[s].astype(F32) * spreads[s]
+    attended = (merged / divisor).astype(BF16)
 
     loads[11].wait()
-    width = half_in.shape[1]
-    other = lax.rem(core + 1, n_tp)
-    half_out[...] = dot(attended, wo[:, pl.ds(pl.multiple_of(other * width, width), width)]).astype(
-        BF16
-    )
+    out_cols = half_in.shape[1]
+    half_out[...] = dot(attended, wo[:, cols(other, out_cols)]).astype(BF16)
     swap = pltpu.make_async_remote_copy(
         src_ref=half_out,
         dst_ref=half_in,
-        send_sem=tp_sem.at[0],
-        recv_sem=tp_sem.at[1],
+        send_sem=tp_sem.at[2],
+        recv_sem=tp_sem.at[3],
         device_id={"tp": other},
         device_id_type=MESH,
     )
     swap.start()
-    mine = dot(attended, wo[:, pl.ds(pl.multiple_of(core * width, width), width)]).astype(BF16)
+    kept = dot(attended, wo[:, cols(core, out_cols)]).astype(BF16)
     swap.wait()
-    mixed_ref[...] = (mine.astype(F32) + half_in[...].astype(F32)).astype(BF16)
+    mixed_ref[...] = (kept.astype(F32) + half_in[...].astype(F32)).astype(BF16)
     for c in sent:
         c.wait_send()
 
 
-def fused(n_kv, n_tp, *args):
+def fused(n_dp, n_kv, n_tp, *args):
     (x, gain, wqn, wqr, wl, wk, kvg, wuk, wuv, wo, cache, rope, lengths) = args
     seqs, rank = x.shape[0], wl.shape[1]
     heads = wqn.shape[1] // NOPE
-    q_cols = wqn.shape[1] + wqr.shape[1] + LANES
     half = wo.shape[1] // n_tp
-    freq = THETA ** (-(np.arange(wqr.shape[1]) % (ROPE // 2)) * 2.0 / ROPE)
+    freq = THETA ** (-(np.arange(LANES) % (ROPE // 2)) * 2.0 / ROPE)
     freq = jnp.asarray(freq.astype(np.float32)[None, :])
     any_spec = pl.BlockSpec(memory_space=pl.ANY)
     vmem = pl.BlockSpec(memory_space=pltpu.VMEM)
 
-    def like(a, *lead):
-        return pltpu.VMEM(tuple(lead) + a.shape, a.dtype)
+    def like(a):
+        return pltpu.VMEM(a.shape, a.dtype)
 
     gain = gain.reshape(1, -1)
     kvg = kvg.reshape(1, -1)
+    wk = wk.T
     return pl.pallas_call(
-        functools.partial(kernel, n_kv, n_tp),
+        functools.partial(kernel, n_dp, n_kv, n_tp),
         out_shape=(
             jax.ShapeDtypeStruct((seqs, half), BF16),
             jax.ShapeDtypeStruct((seqs, rank), BF16),
@@ -382,24 +445,32 @@
             like(gain),
             like(wqn),
             like(wqr),
-            like(wl),
+            pltpu.VMEM((wl.shape[0], rank // n_tp), BF16),
             like(wk),
             like(kvg),
-            like(wuk, n_kv),
-            like(wuv, n_kv),
+            pltpu.VMEM((n_kv, wuk.shape[0], LANES), BF16),
+            pltpu.VMEM((n_kv,) + wuv.shape, BF16),
             like(wo),
             like(cache),
             like(rope),
-            pltpu.VMEM((n_kv, seqs, q_cols), F32),
-            pltpu.VMEM((n_kv, seqs, rank), F32),
-            pltpu.VMEM((n_kv, seqs, wuv.shape[1] + LANES), F32),
+            pltpu.VMEM((seqs, LANES), F32),
+            pltpu.VMEM((n_kv, seqs, 2 * LANES), F32),
+            pltpu.VMEM((n_kv, seqs, 2 * LANES), F32),
+            pltpu.VMEM((n_kv, seqs, rank // n_tp), F32),
+            pltpu.VMEM((n_tp, seqs, rank // n_tp), F32),
+            pltpu.VMEM((n_kv, heads // n_kv * seqs, rank), BF16),
+            pltpu.VMEM((n_kv, seqs, LANES), BF16),
+            pltpu.VMEM((n_kv, seqs, wuv.shape[1]), BF16),
+            pltpu.VMEM((n_kv, seqs, LANES), F32),
             pltpu.VMEM((seqs, half), BF16),
             pltpu.VMEM((seqs, half), BF16),
             pltpu.VMEM((seqs * heads, cache.shape[1]), F32),
             pltpu.SemaphoreType.DMA((12,)),
-            pltpu.SemaphoreType.DMA((5, n_kv - 1)),
-            pltpu.SemaphoreType.DMA((5, n_kv)),
-            pltpu.SemaphoreType.DMA((2,)),
+            pltpu.SemaphoreType.DMA((8, n_kv - 1)),
+            pltpu.SemaphoreType.DMA((8, n_kv)),
+            pltpu.SemaphoreType.DMA((n_dp - 1, n_kv - 1)),
+            pltpu.SemaphoreType.DMA((n_dp, n_kv - 1)),
+            pltpu.SemaphoreType.DMA((4,)),
         ],
         compiler_params=pltpu.CompilerParams(collective_id=0, has_side_effects=True),
     )(lengths, freq, x, gain, wqn, wqr, wl, wk, kvg, wuk, wuv, wo, cache, rope)
@@ -499,12 +570,13 @@
 
 
 def solution(mesh):
-    n_kv, n_tp = mesh.shape["kv"], mesh.shape["tp"]
+    n_dp, n_kv, n_tp = mesh.shape["dp"], mesh.shape["kv"], mesh.shape["tp"]
 
     def body(*args):
         width, rank = args[9].shape[1], args[4].shape[1]
-        if (width // n_tp) % LANES == 0 and (rank // n_kv) % LANES == 0:
-            return fused(n_kv, n_tp, *args)
+        aligned = (width // n_tp) % LANES == 0 and (rank // n_kv) % LANES == 0
+        if aligned and args[2].shape[1] == n_kv * LANES and n_tp == 2:
+            return fused(n_dp, n_kv, n_tp, *args)
         return local(*args)
 
     return jax.shard_map(

time: 51 us -> 34.2 us (0.67)
  Pallas kernels: 44.4 us -> 29.2 us
  local copies, waits for them, and re-layouts: 5.59 us -> 3.92 us
    pallas_call x1, Pallas kernels: 44.4 us -> 29.2 us  [fused(): pl.pallas_call(functools.partial(kernel, n_dp, n_kv, n_tp), out_shape=(ja...]
    unnamed x4 -> x3, local copies, waits for them, and re-layouts: 5.59 us -> 3.92 us
where the time goes in v2:
time: 34.2 us; the launch traced here: 33.8 us
  Pallas kernels  29.2 us (85%)
  local copies, waits for them, and re-layouts  3.92 us (11%)
  between operations  0.64 us (2%)
    pallas_call x1, Pallas kernels, fused(): pl.pallas_call(functools.partial(kernel, n_dp, n_kv, n_tp), out_shape=(ja...  29.2 us
    unnamed x3, local copies, waits for them, and re-layouts  3.92 us

profile of v2, /device:TPU:0, one launch (start us, length us, event | category | flops | bytes accessed | tf_op | source)
XLA Modules:
  0.0 33.8 jit_solution(1224141494501886860)
XLA Ops:
  0.6 29.2 %shard_map.157 = (bf16[16,512]{1,0:T(8,128)(2,1)}, bf16[16,512]{1,0:T(8,128)(2,1)}, bf16[16,32]{1,0:T(8,128)(2,1)}) custom-call(s32[16]{0:T(128)} %len_ref.1, f32[1,128]{1,0:T(1,128)} %constant.2.clone.freq_ref, bf16[16,1024]{1,0:T(8,128)(2,1)} %x_hbm.1, f32[1,1024]{1,0:T(1,128)} %bitcast.4, bf16[1024,512]{1,0:T(8,128)(2,1)} %wqn_hbm.1, ...), custom_call_target="tpu_custom_call" | custom-call | tf_op jit(solution)/shard_map/pallas_call | solution.py:434
  29.9 1.3 %copy.20 = bf16[16,512]{1,0:T(8,128)(2,1)} copy(bf16[16,512]{1,0:T(8,128)(2,1)} %get-tuple-element.6) | data formatting | bytes 32768
  31.2 1.3 %copy.21 = bf16[16,512]{1,0:T(8,128)(2,1)} copy(bf16[16,512]{1,0:T(8,128)(2,1)} %get-tuple-element.7) | data formatting | bytes 32768
  32.5 1.3 %copy.22 = bf16[16,32]{1,0:T(8,128)(2,1)} copy(bf16[16,32]{1,0:T(8,128)(2,1)} %get-tuple-element.8) | data formatting | bytes 2048

commit v3 on v2

--- a/solution.py
+++ b/solution.py
@@ -18,6 +18,7 @@
 THETA = 10000.0
 NEG = -1e30
 LANES = 128
+CHUNKS = 2
 MESH = pl.DeviceIdType.MESH
 BF16 = jnp.bfloat16
 F32 = jnp.float32
@@ -119,11 +120,21 @@
     lat_cols = wl.shape[1]
     block = cache.shape[1]
     rows = wuv_hbm.shape[0]
+    chunks = q_lat.shape[0]
+    span = seqs // chunks
+    count = span * heads
     part = rows // n_dp
 
     def cols(index, width):
         return pl.ds(pl.multiple_of(index * width, width), width)
 
+    barrier = pltpu.get_barrier_semaphore()
+    axes = (("kv", me, n_kv), ("tp", core, n_tp), ("dp", group, n_dp))
+    for name, index, size in axes:
+        for j in range(1, size):
+            pl.semaphore_signal(
+                barrier, inc=1, device_id={name: lax.rem(index + j, size)}, device_id_type=MESH
+            )
     part_rows = cols(group, part)
     pairs = (
         (x_hbm, x),
@@ -140,16 +151,8 @@
         (wo_hbm, wo),
     )
     loads = [pltpu.make_async_copy(s, d, load_sem.at[i]) for i, (s, d) in enumerate(pairs)]
-    for load in loads:
-        load.start()
-
-    barrier = pltpu.get_barrier_semaphore()
-    axes = (("kv", me, n_kv), ("tp", core, n_tp), ("dp", group, n_dp))
-    for name, index, size in axes:
-        for j in range(1, size):
-            pl.semaphore_signal(
-                barrier, inc=1, device_id={name: lax.rem(index + j, size)}, device_id_type=MESH
-            )
+    for i in (0, 1, 4, 2, 3):
+        loads[i].start()
     pl.semaphore_wait(barrier, n_kv - 1 + n_tp - 1 + n_dp - 1)
 
     sent = []
@@ -193,6 +196,8 @@
     rope_own = own_heads * ROPE
     key_part = pltpu.roll(key_pad[...], rope_own, 1)
     loads[2].wait()
+    for i in (5, 7, 6, 8, 9, 10, 11):
+        loads[i].start()
     nope_part = dot(scaled, wqn[...])
     loads[3].wait()
     rope_part = dot(scaled, wqr[...])
@@ -231,13 +236,22 @@
     q_rots[me] = turned
     send(4, lambda p: q_rots.at[me], lambda s: q_rots.at[s])
     q_blocks = jnp.concatenate(
-        [jnp.where(lane // NOPE == h, q_low, 0.0) for h in range(own_heads)], axis=0
+        [
+            jnp.where(lane[:span] // NOPE == h, q_low[c * span : (c + 1) * span], 0.0)
+            for c in range(chunks)
+            for h in range(own_heads)
+        ],
+        axis=0,
     ).astype(BF16)
     loads[7].wait()
     arrive(0, lambda s: wuk.at[s])
+    per_chunk = own_heads * span
     for s in range(n_kv):
-        q_lat[me, :, s * rows : (s + 1) * rows] = dot_nt(q_blocks, wuk[s]).astype(BF16)
-    send(5, lambda p: q_lat.at[me], lambda s: q_lat.at[s])
+        piece = dot_nt(q_blocks, wuk[s]).astype(BF16)
+        for c in range(chunks):
+            q_lat[c, me, :, s * rows : (s + 1) * rows] = piece[c * per_chunk : (c + 1) * per_chunk]
+    for c in range(chunks):
+        send(5 + c, lambda p: q_lat.at[c, me], lambda s: q_lat.at[c, s])
     rope_new = pltpu.roll(turned.astype(F32), LANES - rope_own, 1)
     rnew_ref[...] = rope_new[:, :ROPE].astype(BF16)
 
@@ -273,10 +287,6 @@
     )
     lat_swap.start()
 
-    count = seqs * heads
-    to = lax.broadcasted_iota(jnp.int32, (count, count), 0)
-    frm = lax.broadcasted_iota(jnp.int32, (count, count), 1)
-    order = jnp.where(frm == (to % heads) * seqs + to // heads, 1.0, 0.0).astype(BF16)
     arrive(4, lambda s: q_rots.at[s])
     wide = jnp.concatenate([q_rots[s] for s in range(n_kv)], axis=1).astype(F32)
     shape = (seqs, heads, n_kv * LANES)
@@ -284,117 +294,136 @@
     at = lax.broadcasted_iota(jnp.int32, shape, 2)
     mine = (at // LANES == head // own_heads) & ((at % LANES) // ROPE == head % own_heads)
     r_blocks = jnp.where(mine, jnp.broadcast_to(wide[:, None, :], shape), 0.0)
-    r_blocks = r_blocks.reshape(count, n_kv * LANES).astype(BF16)
+    r_blocks = r_blocks.reshape(seqs * heads, n_kv * LANES).astype(BF16)
     pick_shape = (n_kv * LANES, LANES)
     pick = (
         lax.broadcasted_iota(jnp.int32, pick_shape, 0) % ROPE
         == lax.broadcasted_iota(jnp.int32, pick_shape, 1)
     )
     q_rot_rows = dot(r_blocks, jnp.where(pick, 1.0, 0.0).astype(BF16))
-    arrive(5, lambda s: q_lat.at[s])
-    q_latent = dot(order, q_lat[...].reshape(count, rank))
-
-    loads[8].wait()
-    loads[9].wait()
-    for b in range(seqs):
-        span = slice(b * heads, (b + 1) * heads)
-        scores[span, :] = dot_nt(q_latent[span].astype(BF16), cache[b]) + dot(
-            q_rot_rows[span, :ROPE].astype(BF16), rope[b]
-        )
-
-    loads[6].wait()
-    lat_swap.wait()
-    latent_raw = jnp.concatenate([lat_half[t] for t in range(n_tp)], axis=1) * inv_rms
-    mean_square = jnp.mean(latent_raw * latent_raw, axis=1, keepdims=True)
-    latent_new = (latent_raw * lax.rsqrt(mean_square + EPS) * kvg[...]).astype(BF16)
-    lnew_ref[...] = latent_new
+
+    to = lax.broadcasted_iota(jnp.int32, (count, count), 0)
+    frm = lax.broadcasted_iota(jnp.int32, (count, count), 1)
+    order = jnp.where(frm == (to % heads) * span + to // heads, 1.0, 0.0).astype(BF16)
+    place = me * block + lax.broadcasted_iota(jnp.int32, (count, block), 1)
+    score_scale = (NOPE + ROPE) ** (-0.5)
+    stat_shape = (span, heads, LANES)
+    stat_head = lax.broadcasted_iota(jnp.int32, stat_shape, 1)
+    stat_lane = lax.broadcasted_iota(jnp.int32, stat_shape, 2)
+    width = wuv.shape[2]
+    val_shape = (span, heads, width)
+    own_columns = lax.broadcasted_iota(jnp.int32, val_shape, 2) // V_DIM == (
+        lax.broadcasted_iota(jnp.int32, val_shape, 1)
+    )
 
     def rows_of(u):
-        return jnp.broadcast_to(u[:, None, :], (seqs, heads, u.shape[1])).reshape(
+        return jnp.broadcast_to(u[:, None, :], (span, heads, u.shape[1])).reshape(
             count, u.shape[1]
         )
 
-    new_rows = rows_of(latent_new.astype(F32))
-    key_rows = rows_of(rope_new)
-    own = jnp.sum(q_latent * new_rows, axis=1, keepdims=True)
-    own = own + jnp.sum(q_rot_rows * key_rows, axis=1, keepdims=True)
-
-    score_scale = (NOPE + ROPE) ** (-0.5)
-    limit = jnp.concatenate(
-        [jnp.full((heads, block), len_ref[b], jnp.int32) for b in range(seqs)], axis=0
-    )
-    place = me * block + lax.broadcasted_iota(jnp.int32, (count, block), 1)
-    newslot = place == limit
-    usable = place <= limit
-    masked = jnp.where(usable, jnp.where(newslot, own, scores[...]) * score_scale, NEG)
-    local_max = jnp.max(masked, axis=1, keepdims=True)
-    weights = jnp.where(usable, jnp.exp(masked - local_max), 0.0)
-    totals = jnp.sum(weights, axis=1, keepdims=True)
-    rounded = weights.astype(BF16).astype(F32)
-    own_weight = jnp.sum(jnp.where(newslot, rounded, 0.0), axis=1, keepdims=True)
-    cache_weights = jnp.where(newslot, 0.0, rounded)
-    weighted = jnp.concatenate(
-        [
-            dot(cache_weights[b * heads : (b + 1) * heads].astype(BF16), cache[b])
-            for b in range(seqs)
-        ],
-        axis=0,
-    )
-    weighted = (weighted + own_weight * new_rows).astype(BF16)
-
-    shape = (seqs, heads, LANES)
-    head = lax.broadcasted_iota(jnp.int32, shape, 1)
-    at = lax.broadcasted_iota(jnp.int32, shape, 2)
-    stats = jnp.where(
-        at == head, jnp.broadcast_to(local_max, (count, LANES)).reshape(shape), 0.0
-    ) + jnp.where(
-        at == head + LANES // 2, jnp.broadcast_to(totals, (count, LANES)).reshape(shape), 0.0
-    )
-    stat_in[me] = jnp.sum(stats, axis=1)
-    send(6, lambda p: stat_in.at[me], lambda s: stat_in.at[s])
-    loads[10].wait()
-    for j in range(1, n_dp):
-        source_group = lax.rem(group + j, n_dp)
-        their_rows = cols(source_group, part)
-        for i in range(1, n_kv):
-            source = lax.rem(me + i, n_kv)
-            pltpu.make_async_remote_copy(
-                src_ref=wuv.at[source, their_rows],
-                dst_ref=wuv.at[source, their_rows],
-                send_sem=dp_send.at[j - 1, i - 1],
-                recv_sem=dp_recv.at[source_group, i - 1],
-                device_id={"dp": source_group},
-                device_id_type=MESH,
-            ).wait_recv()
-    values = dot(weighted, wuv[...].reshape(rank, wuv.shape[2]))
-    width = values.shape[1]
-    values = values.reshape(seqs, heads, width)
-    head = lax.broadcasted_iota(jnp.int32, values.shape, 1)
-    at = lax.broadcasted_iota(jnp.int32, values.shape, 2)
-    val_in[me] = jnp.sum(jnp.where(at // V_DIM == head, values, 0.0), axis=1).astype(BF16)
-    send(7, lambda p: val_in.at[me], lambda s: val_in.at[s])
-
-    arrive(6, lambda s: stat_in.at[s])
-    maxima = [stat_in[s] for s in range(n_kv)]
-    sums = [pltpu.roll(m, LANES // 2, 1) for m in maxima]
-    highest = functools.reduce(jnp.maximum, maxima)
-    factors = [jnp.exp(m - highest) for m in maxima]
-    whole = functools.reduce(jnp.add, [f * t for f, t in zip(factors, sums)])
-    at = lax.broadcasted_iota(jnp.int32, (seqs, width), 1)
+    for c in range(chunks):
+        first = c * span
+        arrive(5 + c, lambda s: q_lat.at[c, s])
+        q_latent = dot(order, q_lat[c].reshape(count, rank))
+        q_turn = q_rot_rows[first * heads : (first + span) * heads]
+        if c == 0:
+            loads[8].wait()
+            loads[9].wait()
+        for b in range(span):
+            some = slice(b * heads, (b + 1) * heads)
+            scores[some, :] = dot_nt(q_latent[some].astype(BF16), cache[first + b]) + dot(
+                q_turn[some, :ROPE].astype(BF16), rope[first + b]
+            )
+        if c == 0:
+            loads[6].wait()
+            lat_swap.wait()
+            latent_raw = jnp.concatenate([lat_half[t] for t in range(n_tp)], axis=1) * inv_rms
+            mean_square = jnp.mean(latent_raw * latent_raw, axis=1, keepdims=True)
+            latent_new = latent_raw * lax.rsqrt(mean_square + EPS) * kvg[...]
+            latent_new = latent_new.astype(BF16)
+            lnew_ref[...] = latent_new
+            latent_wide = latent_new.astype(F32)
+
+        new_rows = rows_of(latent_wide[first : first + span])
+        key_rows = rows_of(rope_new[first : first + span])
+        own = jnp.sum(q_latent * new_rows, axis=1, keepdims=True)
+        own = own + jnp.sum(q_turn * key_rows, axis=1, keepdims=True)
+
+        limit = jnp.concatenate(
+            [jnp.full((heads, block), len_ref[first + b], jnp.int32) for b in range(span)], axis=0
+        )
+        newslot = place == limit
+        usable = place <= limit
+        masked = jnp.where(usable, jnp.where(newslot, own, scores[...]) * score_scale, NEG)
+        local_max = jnp.max(masked, axis=1, keepdims=True)
+        weights = jnp.where(usable, jnp.exp(masked - local_max), 0.0)
+        totals = jnp.sum(weights, axis=1, keepdims=True)
+        rounded = weights.astype(BF16).astype(F32)
+        own_weight = jnp.sum(jnp.where(newslot, rounded, 0.0), axis=1, keepdims=True)
+        cache_weights = jnp.where(newslot, 0.0, rounded)
+        stats = jnp.where(
+            stat_lane == stat_head,
+            jnp.broadcast_to(local_max, (count, LANES)).reshape(stat_shape),
+            0.0,
+        ) + jnp.where(
+            stat_lane == stat_head + LANES // 2,
+            jnp.broadcast_to(totals, (count, LANES)).reshape(stat_shape),
+            0.0,
+        )
+        stat_in[c, me] = jnp.sum(stats, axis=1)
+        send(7 + c, lambda p: stat_in.at[c, me], lambda s: stat_in.at[c, s])
+        weighted = jnp.concatenate(
+            [
+                dot(cache_weights[b * heads : (b + 1) * heads].astype(BF16), cache[first + b])
+                for b in range(span)
+            ],
+            axis=0,
+        )
+        weighted = (weighted + own_weight * new_rows).astype(BF16)
+
+        if c == 0:
+            loads[10].wait()
+            for j in range(1, n_dp):
+                source_group = lax.rem(group + j, n_dp)
+                their_rows = cols(source_group, part)
+                for i in range(1, n_kv):
+                    source = lax.rem(me + i, n_kv)
+                    pltpu.make_async_remote_copy(
+                        src_ref=wuv.at[source, their_rows],
+                        dst_ref=wuv.at[source, their_rows],
+                        send_sem=dp_send.at[j - 1, i - 1],
+                        recv_sem=dp_recv.at[source_group, i - 1],
+                        device_id={"dp": source_group},
+                        device_id_type=MESH,
+                    ).wait_recv()
+        values = dot(weighted, wuv[...].reshape(rank, width)).reshape(val_shape)
+        val_in[c, me] = jnp.sum(jnp.where(own_columns, values, 0.0), axis=1).astype(BF16)
+        send(9 + c, lambda p: val_in.at[c, me], lambda s: val_in.at[c, s])
+
+    at = lax.broadcasted_iota(jnp.int32, (span, width), 1)
 
     def spread(u):
-        out = jnp.broadcast_to(u[:, :1], (seqs, width))
+        out = jnp.broadcast_to(u[:, :1], (span, width))
         for h in range(1, heads):
             out = jnp.where(at // V_DIM == h, u[:, h : h + 1], out)
         return out
 
-    spreads = [spread(f) for f in factors]
-    divisor = spread(whole)
-    arrive(7, lambda s: val_in.at[s])
-    merged = val_in[0].astype(F32) * spreads[0]
-    for s in range(1, n_kv):
-        merged = merged + val_in[s].astype(F32) * spreads[s]
-    attended = (merged / divisor).astype(BF16)
+    merged_chunks = []
+    for c in range(chunks):
+        arrive(7 + c, lambda s: stat_in.at[c, s])
+        maxima = [stat_in[c, s] for s in range(n_kv)]
+        sums = [pltpu.roll(m, LANES // 2, 1) for m in maxima]
+        highest = functools.reduce(jnp.maximum, maxima)
+        factors = [jnp.exp(m - highest) for m in maxima]
+        whole = functools.reduce(jnp.add, [f * t for f, t in zip(factors, sums)])
+        spreads = [spread(f) for f in factors]
+        divisor = spread(whole)
+        arrive(9 + c, lambda s: val_in.at[c, s])
+        merged = val_in[c, 0].astype(F32) * spreads[0]
+        for s in range(1, n_kv):
+            merged = merged + val_in[c, s].astype(F32) * spreads[s]
+        merged_chunks.append(merged / divisor)
+    attended = jnp.concatenate(merged_chunks, axis=0).astype(BF16)
 
     loads[11].wait()
     out_cols = half_in.shape[1]
@@ -415,6 +444,17 @@
         c.wait_send()
 
 
+def hand_out(*refs):
+    n = (len(refs) - 1) // 3
+    ins, outs, held, sem = refs[:n], refs[n : 2 * n], refs[2 * n : 3 * n], refs[-1]
+    for step, (frm, to) in enumerate(((ins, held), (held, outs))):
+        copies = [pltpu.make_async_copy(frm[i], to[i], sem.at[step, i]) for i in range(n)]
+        for copy in copies:
+            copy.start()
+        for copy in copies:
+            copy.wait()
+
+
 def fused(n_dp, n_kv, n_tp, *args):
     (x, gain, wqn, wqr, wl, wk, kvg, wuk, wuv, wo, cache, rope, lengths) = args
     seqs, rank = x.shape[0], wl.shape[1]
@@ -431,7 +471,7 @@
     gain = gain.reshape(1, -1)
     kvg = kvg.reshape(1, -1)
     wk = wk.T
-    return pl.pallas_call(
+    outs = pl.pallas_call(
         functools.partial(kernel, n_dp, n_kv, n_tp),
         out_shape=(
             jax.ShapeDtypeStruct((seqs, half), BF16),
@@ -458,22 +498,29 @@
             pltpu.VMEM((n_kv, seqs, 2 * LANES), F32),
             pltpu.VMEM((n_kv, seqs, rank // n_tp), F32),
             pltpu.VMEM((n_tp, seqs, rank // n_tp), F32),
-            pltpu.VMEM((n_kv, heads // n_kv * seqs, rank), BF16),
+            pltpu.VMEM((CHUNKS, n_kv, heads // n_kv * seqs // CHUNKS, rank), BF16),
             pltpu.VMEM((n_kv, seqs, LANES), BF16),
-            pltpu.VMEM((n_kv, seqs, wuv.shape[1]), BF16),
-            pltpu.VMEM((n_kv, seqs, LANES), F32),
+            pltpu.VMEM((CHUNKS, n_kv, seqs // CHUNKS, wuv.shape[1]), BF16),
+            pltpu.VMEM((CHUNKS, n_kv, seqs // CHUNKS, LANES), F32),
             pltpu.VMEM((seqs, half), BF16),
             pltpu.VMEM((seqs, half), BF16),
-            pltpu.VMEM((seqs * heads, cache.shape[1]), F32),
+            pltpu.VMEM((seqs * heads // CHUNKS, cache.shape[1]), F32),
             pltpu.SemaphoreType.DMA((12,)),
-            pltpu.SemaphoreType.DMA((8, n_kv - 1)),
-            pltpu.SemaphoreType.DMA((8, n_kv)),
+            pltpu.SemaphoreType.DMA((5 + 3 * CHUNKS, n_kv - 1)),
+            pltpu.SemaphoreType.DMA((5 + 3 * CHUNKS, n_kv)),
             pltpu.SemaphoreType.DMA((n_dp - 1, n_kv - 1)),
             pltpu.SemaphoreType.DMA((n_dp, n_kv - 1)),
             pltpu.SemaphoreType.DMA((4,)),
         ],
         compiler_params=pltpu.CompilerParams(collective_id=0, has_side_effects=True),
     )(lengths, freq, x, gain, wqn, wqr, wl, wk, kvg, wuk, wuv, wo, cache, rope)
+    return pl.pallas_call(
+        hand_out,
+        out_shape=tuple(jax.ShapeDtypeStruct(o.shape, o.dtype) for o in outs),
+        in_specs=[any_spec] * len(outs),
+        out_specs=(any_spec,) * len(outs),
+        scratch_shapes=[like(o) for o in outs] + [pltpu.SemaphoreType.DMA((2, len(outs)))],
+    )(*outs)
 
 
 def local(

time: 34.2 us -> 32.8 us (0.959)
  local copies, waits for them, and re-layouts: 3.92 us -> 0 us
  Pallas kernels: 29.2 us -> 31.9 us
    unnamed x3 -> x0, local copies, waits for them, and re-layouts: 3.92 us -> none
    pallas_call x0 -> x1, Pallas kernels: none -> 1.4 us  [fused(): pl.pallas_call(hand_out, out_shape=tuple((jax.ShapeDtypeStruct(o.shape, o...]
    pallas_call x1, Pallas kernels: 29.2 us -> 30.5 us  [fused(): pl.pallas_call(functools.partial(kernel, n_dp, n_kv, n_tp), out_shape=(ja...]
where the time goes in v3:
time: 32.8 us; the launch traced here: 32.6 us
  Pallas kernels  31.9 us (97%)
  between operations  0.64 us (2%)
    pallas_call x1, Pallas kernels, fused(): pl.pallas_call(functools.partial(kernel, n_dp, n_kv, n_tp), out_shape=(ja...  30.5 us
    pallas_call x1, Pallas kernels, fused(): pl.pallas_call(hand_out, out_shape=tuple((jax.ShapeDtypeStruct(o.shape, o...  1.4 us

profile of v3, /device:TPU:0, one launch (start us, length us, event | category | flops | bytes accessed | tf_op | source)
XLA Modules:
  0.0 32.6 jit_solution(16882866511325005665)
XLA Ops:
  0.6 30.5 %shard_map.157 = (bf16[16,512]{1,0:T(8,128)(2,1)}, bf16[16,512]{1,0:T(8,128)(2,1)}, bf16[16,32]{1,0:T(8,128)(2,1)}) custom-call(s32[16]{0:T(128)} %len_ref.1, f32[1,128]{1,0:T(1,128)} %constant.2.clone.freq_ref, bf16[16,1024]{1,0:T(8,128)(2,1)} %x_hbm.1, f32[1,1024]{1,0:T(1,128)} %bitcast.4, bf16[1024,512]{1,0:T(8,128)(2,1)} %wqn_hbm.1, ...), custom_call_target="tpu_custom_call" | custom-call | tf_op jit(solution)/shard_map/pallas_call | solution.py:474
  31.2 1.4 %shard_map.158 = (bf16[16,512]{1,0:T(8,128)(2,1)}, bf16[16,512]{1,0:T(8,128)(2,1)}, bf16[16,32]{1,0:T(8,128)(2,1)}) custom-call(bf16[16,512]{1,0:T(8,128)(2,1)} %get-tuple-element.6.refs_0_, bf16[16,512]{1,0:T(8,128)(2,1)} %get-tuple-element.7.refs_1_, bf16[16,32]{1,0:T(8,128)(2,1)} %get-tuple-element.8.refs_2_), custom_call_target="tpu_custom_call" | custom-call | tf_op jit(solution)/shard_map/pallas_call | solution.py:517

commit v4 on v3

--- a/solution.py
+++ b/solution.py
@@ -183,7 +183,32 @@
                 device_id_type=MESH,
             ).wait_recv()
 
-    send(0, lambda p: wuk_hbm.at[:, cols(p, LANES)], lambda s: wuk.at[s])
+    def dp_copy(which, buf, peer, j, i, owner):
+        piece = buf.at[lax.rem(me + i, n_kv), cols(owner, part)]
+        return pltpu.make_async_remote_copy(
+            src_ref=piece,
+            dst_ref=piece,
+            send_sem=dp_send.at[which, j - 1, i - 1],
+            recv_sem=dp_recv.at[which, owner, i - 1],
+            device_id={"dp": peer},
+            device_id_type=MESH,
+        )
+
+    def forward(which, phase, buf):
+        arrive(phase, lambda s: buf.at[s, part_rows])
+        for j in range(1, n_dp):
+            for i in range(1, n_kv):
+                copy = dp_copy(which, buf, lax.rem(group + j, n_dp), j, i, group)
+                copy.start()
+                sent.append(copy)
+
+    def join(which, buf):
+        for j in range(1, n_dp):
+            owner = lax.rem(group + j, n_dp)
+            for i in range(1, n_kv):
+                dp_copy(which, buf, owner, j, i, owner).wait_recv()
+
+    send(0, lambda p: wuk_hbm.at[part_rows, cols(p, LANES)], lambda s: wuk.at[s, part_rows])
 
     loads[0].wait()
     loads[1].wait()
@@ -224,6 +249,7 @@
     cosine = jnp.cos(angles)
     sine = jnp.sin(angles)
 
+    forward(0, 0, wuk)
     arrive(1, lambda s: q_in.at[s])
     total_q = q_in[0]
     for s in range(1, n_kv):
@@ -244,7 +270,7 @@
         axis=0,
     ).astype(BF16)
     loads[7].wait()
-    arrive(0, lambda s: wuk.at[s])
+    join(0, wuk)
     per_chunk = own_heads * span
     for s in range(n_kv):
         piece = dot_nt(q_blocks, wuk[s]).astype(BF16)
@@ -255,21 +281,7 @@
     rope_new = pltpu.roll(turned.astype(F32), LANES - rope_own, 1)
     rnew_ref[...] = rope_new[:, :ROPE].astype(BF16)
 
-    arrive(2, lambda s: wuv.at[s, part_rows])
-    for j in range(1, n_dp):
-        peer = lax.rem(group + j, n_dp)
-        for i in range(1, n_kv):
-            source = lax.rem(me + i, n_kv)
-            copy = pltpu.make_async_remote_copy(
-                src_ref=wuv.at[source, part_rows],
-                dst_ref=wuv.at[source, part_rows],
-                send_sem=dp_send.at[j - 1, i - 1],
-                recv_sem=dp_recv.at[group, i - 1],
-                device_id={"dp": peer},
-                device_id_type=MESH,
-            )
-            copy.start()
-            sent.append(copy)
+    forward(1, 2, wuv)
 
     arrive(3, lambda s: lat_in.at[s])
     total_l = lat_in[0]
@@ -383,19 +395,7 @@
 
         if c == 0:
             loads[10].wait()
-            for j in range(1, n_dp):
-                source_group = lax.rem(group + j, n_dp)
-                their_rows = cols(source_group, part)
-                for i in range(1, n_kv):
-                    source = lax.rem(me + i, n_kv)
-                    pltpu.make_async_remote_copy(
-                        src_ref=wuv.at[source, their_rows],
-                        dst_ref=wuv.at[source, their_rows],
-                        send_sem=dp_send.at[j - 1, i - 1],
-                        recv_sem=dp_recv.at[source_group, i - 1],
-                        device_id={"dp": source_group},
-                        device_id_type=MESH,
-                    ).wait_recv()
+            join(1, wuv)
         values = dot(weighted, wuv[...].reshape(rank, width)).reshape(val_shape)
         val_in[c, me] = jnp.sum(jnp.where(own_columns, values, 0.0), axis=1).astype(BF16)
         send(9 + c, lambda p: val_in.at[c, me], lambda s: val_in.at[c, s])
@@ -508,8 +508,8 @@
             pltpu.SemaphoreType.DMA((12,)),
             pltpu.SemaphoreType.DMA((5 + 3 * CHUNKS, n_kv - 1)),
             pltpu.SemaphoreType.DMA((5 + 3 * CHUNKS, n_kv)),
-            pltpu.SemaphoreType.DMA((n_dp - 1, n_kv - 1)),
-            pltpu.SemaphoreType.DMA((n_dp, n_kv - 1)),
+            pltpu.SemaphoreType.DMA((2, n_dp - 1, n_kv - 1)),
+            pltpu.SemaphoreType.DMA((2, n_dp, n_kv - 1)),
             pltpu.SemaphoreType.DMA((4,)),
         ],
         compiler_params=pltpu.CompilerParams(collective_id=0, has_side_effects=True),

time: 32.8 us -> 30.9 us (0.942)
  Pallas kernels: 31.9 us -> 30 us
    pallas_call x1, Pallas kernels: 30.5 us -> 28.6 us  [fused(): pl.pallas_call(functools.partial(kernel, n_dp, n_kv, n_tp), out_shape=(ja...]
where the time goes in v4:
time: 30.9 us; the launch traced here: 30.6 us
  Pallas kernels  30 us (97%)
  between operations  0.64 us (2%)
    pallas_call x1, Pallas kernels, fused(): pl.pallas_call(functools.partial(kernel, n_dp, n_kv, n_tp), out_shape=(ja...  28.6 us
    pallas_call x1, Pallas kernels, fused(): pl.pallas_call(hand_out, out_shape=tuple((jax.ShapeDtypeStruct(o.shape, o...  1.4 us

profile of v4, /device:TPU:0, one launch (start us, length us, event | category | flops | bytes accessed | tf_op | source)
XLA Modules:
  0.0 30.6 jit_solution(17121395268201430797)
XLA Ops:
  0.6 28.6 %shard_map.157 = (bf16[16,512]{1,0:T(8,128)(2,1)}, bf16[16,512]{1,0:T(8,128)(2,1)}, bf16[16,32]{1,0:T(8,128)(2,1)}) custom-call(s32[16]{0:T(128)} %len_ref.1, f32[1,128]{1,0:T(1,128)} %constant.2.clone.freq_ref, bf16[16,1024]{1,0:T(8,128)(2,1)} %x_hbm.1, f32[1,1024]{1,0:T(1,128)} %bitcast.4, bf16[1024,512]{1,0:T(8,128)(2,1)} %wqn_hbm.1, ...), custom_call_target="tpu_custom_call" | custom-call | tf_op jit(solution)/shard_map/pallas_call | solution.py:474
  29.2 1.4 %shard_map.158 = (bf16[16,512]{1,0:T(8,128)(2,1)}, bf16[16,512]{1,0:T(8,128)(2,1)}, bf16[16,32]{1,0:T(8,128)(2,1)}) custom-call(bf16[16,512]{1,0:T(8,128)(2,1)} %get-tuple-element.6.refs_0_, bf16[16,512]{1,0:T(8,128)(2,1)} %get-tuple-element.7.refs_1_, bf16[16,32]{1,0:T(8,128)(2,1)} %get-tuple-element.8.refs_2_), custom_call_target="tpu_custom_call" | custom-call | tf_op jit(solution)/shard_map/pallas_call | solution.py:517
